TPU v7x, 32 devices: a whole 2x2x4 slice. The times are simulated.
32 devices in a mesh: ep: 8 (over z, y), tp: 4 (over x, core).
Axes of the slice: x: 2, y: 2, z: 4, core: 2. Of those that a mesh axis runs over, the one named last changes fastest.
Arguments:
- tokens: bfloat16 [128, 2048], P('ep'), may hold values from -6 to 6
- norm_gain: float32 [2048], replicated, may hold values from 0.1 to 1.9
- query_weight: bfloat16 [2048, 1024], P(None, 'tp'), may hold values from -0.21875 to 0.21875
- key_weight: bfloat16 [2048, 512], P(None, 'tp'), may hold values from -0.125 to 0.125
- value_weight: bfloat16 [2048, 512], P(None, 'tp'), may hold values from -0.125 to 0.125
- output_weight: bfloat16 [1024, 2048], P('tp'), may hold values from -0.1875 to 0.1875
- head_gain: float32 [128], replicated, may hold values from 0.1 to 1.9
- lambdas: float32 [8], P('tp'), may hold values from 0.3 to 0.8
- key_cache: bfloat16 [128, 1024, 4, 128], P('ep', None, 'tp')
- value_cache: bfloat16 [128, 1024, 4, 128], P('ep', None, 'tp'), may hold values from -6 to 6
- lengths: int32 [128], P('ep'), may hold values from 128 to 1024, as said below
- ffn_gain: float32 [2048], replicated, may hold values from 0.1 to 1.9
- routes: int32 [128, 4], P('ep'), may hold values from 0 to 7, all different within a row; in each aligned block of 16 rows (0 to 15, 16 to 31, ...) at most 16 rows name the same one
- route_weight: float32 [128, 4], P('ep'), may hold values from 0.1 to 1
- expert_gate: bfloat16 [8, 2048, 1024], P('ep', None, 'tp'), may hold values from -0.125 to 0.125
- expert_up: bfloat16 [8, 2048, 1024], P('ep', None, 'tp'), may hold values from -0.125 to 0.125
- expert_down: bfloat16 [8, 1024, 2048], P('ep', 'tp'), may hold values from -0.1875 to 0.1875
- dense_gate: bfloat16 [2048, 2048], P('tp'), may hold values from -0.125 to 0.125
- dense_up: bfloat16 [2048, 2048], P('tp'), may hold values from -0.125 to 0.125
- dense_down: bfloat16 [2048, 2048], P('tp'), may hold values from -0.1875 to 0.1875
- gate_vector: float32 [2048], P('tp')
Outputs:
- layer_out: bfloat16 [128, 2048], P('ep', 'tp')
Inputs may be any that keep to these rules, and one draw needn't show every extreme that they name: `routes`: each row names 4 different experts. Among the rows of one index of ep no expert is named by more than 16 rows, a bound that some block reaches. `lengths`: some sequence has length 1024. Cached positions at or past a sequence's length are not read.
All inputs are finite; a program needn't handle non-finite values.
Results may differ from a plain program's by a relative error of at most 0.015.
The roundings to bfloat16 on the way count: a program that leaves them out, or rounds other values in their place, can miss the bound.
Values may be sent and summed in bfloat16 or wider, within the bound.
A program may use at most 128 MiB of HBM per device.

v0:
```python
import functools

import jax
import jax.numpy as jnp
from jax import lax
from jax.experimental import pallas as pl
from jax.experimental.pallas import tpu as pltpu
from jax.sharding import PartitionSpec as P

HEADS = 8
KV_HEADS = 4
DQK = 64
DV = 128
TOPK = 4
SEQ_CHUNK = 4

epsilon = 1e-06
F32 = jnp.float32
BF16 = jnp.bfloat16
MESH = pl.DeviceIdType.MESH


def rms_scale(values, gain):
    return values * lax.rsqrt(jnp.mean(values * values, axis=-1, keepdims=True) + epsilon) * gain


def silu(v):
    return v / (1.0 + jnp.exp(-v))


def dot(a, b):
    return jnp.dot(a, b, preferred_element_type=F32)


def dot_nt(a, b):
    return lax.dot_general(a, b, (((1,), (1,)), ((), ())), preferred_element_type=F32)


def layer_kernel(
    n_ep, n_tp,
    lengths, lambdas,
    tokens, norm_gain, head_gain, ffn_gain, gate_vector, routes_t, weight_t,
    wq, wk, wv, wo, key_cache, value_cache, wg, wu, wd, dg, du, dd,
    out,
    wq_v, wk_v, wv_v, wo_v, key_v, value_v, wg_v, wu_v, wd_v, dg_v, du_v, dd_v,
    q_rows, k_rows, v_rows, mix,
    ar_send, ar_recv, residual, gathered,
    d_send, d_recv, l_send, l_recv,
    p_send, n_recv, x_send, x_recv, e_send, e_recv,
    load_sem, key_sem, value_sem, wd_sem, dd_sem,
    ar_ss, ar_rs, ag_ss, ag_rs, fw_ss, fw_rs, ds_ss, ds_rs, lg_ss, lg_rs, p_ss, p_rs, x_ss, x_rs, e_ss, e_rs,
    pair_ss,
):
    me = lax.axis_index("ep")
    mt = lax.axis_index("tp")
    n_seq, width = tokens.shape
    cache_len = key_cache.shape[1]
    cols = width // n_tp
    half = width // 2
    side = lax.rem(mt, 2)
    partner = mt + 1 - 2 * side
    far = mt // 2
    n_far = n_tp // 2
    inner = lax.rem(me, 2)
    across = me + 1 - 2 * inner
    outer = me // 2
    n_outer = n_ep // 2

    def ascending(k):
        return k + jnp.where(k >= outer, 1, 0)

    def descending(k):
        v = n_outer - 1 - k
        return v - jnp.where(v <= outer, 1, 0)

    def near_first(k):
        return jnp.where(2 * outer < n_outer, ascending(k), descending(k))

    def far_first(k):
        return jnp.where(2 * outer < n_outer, descending(k), ascending(k))

    def group_at(n):
        k = n // 2
        o = jnp.where(k < n_outer - 1, far_first(k), outer)
        return 2 * o + jnp.where(lax.rem(n, 2) == 0, 1 - inner, inner)

    def load(src, dst, sem):
        copy = pltpu.make_async_copy(src, dst, sem)
        copy.start()
        return copy

    first = [load(wq, wq_v, load_sem.at[0]), load(wk, wk_v, load_sem.at[1]), load(wv, wv_v, load_sem.at[2])]
    n_chunk = n_seq // SEQ_CHUNK

    def cache_copies(i):
        rows = pl.ds(i * SEQ_CHUNK, SEQ_CHUNK)
        return (
            pltpu.make_async_copy(key_cache.at[rows], key_v.at[rows], key_sem.at[i]),
            pltpu.make_async_copy(value_cache.at[rows], value_v.at[rows], value_sem.at[i]),
        )

    for i in range(n_chunk):
        for copy in cache_copies(i):
            copy.start()
    wo_copy = load(wo, wo_v, load_sem.at[3])
    barrier = pltpu.get_barrier_semaphore()
    for d in range(1, n_tp):
        pl.semaphore_signal(barrier, inc=1, device_id={"tp": lax.rem(mt + d, n_tp)}, device_id_type=MESH)

    @pl.loop(1, n_ep)
    def _(d):
        pl.semaphore_signal(barrier, inc=1, device_id={"ep": lax.rem(me + d, n_ep)}, device_id_type=MESH)

    wide = tokens[...].astype(F32)
    normed = rms_scale(wide, norm_gain[...]).astype(BF16)
    for copy in first:
        copy.wait()
    q = dot(normed, wq_v[...]).astype(BF16).astype(F32)
    k_rows[:, 0, :] = dot(normed, wk_v[...]).astype(BF16).astype(F32)
    v_rows[:, 0, :] = dot(normed, wv_v[...]).astype(BF16).astype(F32)
    group = q.shape[1] // (2 * DQK)
    lane = lax.broadcasted_iota(jnp.int32, (n_seq, 2 * DQK), 1)
    q_rows[...] = jnp.zeros_like(q_rows)
    for h in range(group):
        qh = q[:, h * 2 * DQK:(h + 1) * 2 * DQK]
        q_rows[:, h, :] = jnp.where(lane < DQK, qh, 0.0)
        q_rows[:, 4 + h, :] = jnp.where(lane >= DQK, qh, 0.0)
    row_id = lax.broadcasted_iota(jnp.int32, (8, 1), 0)
    lam = jnp.zeros((8, 1), F32)
    for h in range(group):
        lam = jnp.where(row_id == h, lambdas[h], lam)
    position = lax.broadcasted_iota(jnp.int32, (8, cache_len), 1)
    scale = DQK ** (-0.5)

    @pl.loop(0, n_chunk)
    def _(i):
        for copy in cache_copies(i):
            copy.wait()
        seqs = [i * SEQ_CHUNK + j for j in range(SEQ_CHUNK)]
        qs = [q_rows[n] for n in seqs]
        raw = [dot_nt(qn.astype(BF16), key_v[n]) for qn, n in zip(qs, seqs)]
        own = [jnp.sum(qn * k_rows[n], axis=-1, keepdims=True) * scale for qn, n in zip(qs, seqs)]
        scores = [jnp.where(position < lengths[n], r * scale, -jnp.inf) for r, n in zip(raw, seqs)]
        top = [jnp.maximum(jnp.max(r, axis=-1, keepdims=True), o) for r, o in zip(scores, own)]
        e = [jnp.exp(r - t) for r, t in zip(scores, top)]
        own_e = [jnp.exp(o - t) for o, t in zip(own, top)]
        inv = [1.0 / (jnp.sum(en, axis=-1, keepdims=True) + o) for en, o in zip(e, own_e)]
        p = [en * v for en, v in zip(e, inv)]
        po = [jnp.broadcast_to(o * v, (8, DV)) for o, v in zip(own_e, inv)]
        w = [(pn - lam * pltpu.roll(pn, 4, 0)).astype(BF16) for pn in p]
        own_w = [(pn - lam * pltpu.roll(pn, 4, 0)).astype(BF16).astype(F32) for pn in po]
        mixed = [dot(wn, value_v[n]) + ow * v_rows[n] for wn, ow, n in zip(w, own_w, seqs)]
        for n, m in zip(seqs, mixed):
            mix[n] = m

    dense_in = [load(dg, dg_v, load_sem.at[4]), load(du, du_v, load_sem.at[5])]
    dense_out_copies = [load(dd.at[:, pl.ds(j * cols, cols)], dd_v.at[j], dd_sem.at[j]) for j in range(n_tp)]
    expert_in = [load(wg, wg_v, load_sem.at[6]), load(wu, wu_v, load_sem.at[7])]
    expert_out = [load(wd.at[:, pl.ds(j * cols, cols)], wd_v.at[j], wd_sem.at[j]) for j in range(n_tp)]

    heads = [rms_scale(mix[:, h, :], head_gain[...]).astype(BF16) for h in range(group)]
    wo_copy.wait()
    partial = dot(heads[0], wo_v[0:DV, :])
    for h in range(1, group):
        partial = partial + dot(heads[h], wo_v[h * DV:(h + 1) * DV, :])
    ar_send[...] = partial.astype(BF16)

    pl.semaphore_wait(barrier, n_tp - 1 + n_ep - 1)

    def ar_copy(d):
        peer = lax.rem(mt + d, n_tp)
        return pltpu.make_async_remote_copy(
            ar_send, ar_recv.at[mt], ar_ss.at[peer], ar_rs.at[mt], device_id={"tp": peer}, device_id_type=MESH
        )

    def ar_arrival(d):
        peer = lax.rem(mt + d, n_tp)
        return pltpu.make_async_remote_copy(
            ar_send, ar_recv.at[peer], ar_ss.at[peer], ar_rs.at[peer], device_id={"tp": peer}, device_id_type=MESH
        )

    for d in range(1, n_tp):
        ar_copy(d).start()
    attention = ar_send[...].astype(F32)
    for d in range(1, n_tp):
        ar_arrival(d).wait_recv()
        attention = attention + ar_recv[lax.rem(mt + d, n_tp)].astype(F32)
    res = wide + attention
    for j in range(n_tp):
        residual[j] = res[:, j * cols:(j + 1) * cols]
    ffn = rms_scale(res, ffn_gain[...]).astype(BF16)
    gathered[0, me] = ffn[:, :half]
    gathered[1, me] = ffn[:, half:]

    def ag_piece(peer, s, send_sem):
        return pltpu.make_async_remote_copy(
            gathered.at[side, s], gathered.at[side, s], send_sem, ag_rs.at[s],
            device_id={"ep": peer}, device_id_type=MESH,
        )

    def ag_copy(k):
        peer = 2 * far_first(k) + inner
        return ag_piece(peer, me, ag_ss.at[peer])

    def pair_copy(s):
        return ag_piece(across, s, pair_ss.at[s])

    def ag_arrival(s):
        return ag_piece(across, s, ag_ss.at[s])

    def fw_copy(s):
        return pltpu.make_async_remote_copy(
            gathered.at[side, s], gathered.at[side, s], fw_ss.at[s], fw_rs.at[s],
            device_id={"tp": partner}, device_id_type=MESH,
        )

    def fw_arrival(s):
        return pltpu.make_async_remote_copy(
            gathered.at[1 - side, s], gathered.at[1 - side, s], fw_ss.at[s], fw_rs.at[s],
            device_id={"tp": partner}, device_id_type=MESH,
        )

    pair_copy(me).start()

    @pl.loop(0, n_outer - 1)
    def _(k):
        ag_copy(k).start()

    for copy in dense_in:
        copy.wait()
    hidden = (silu(dot_nt(ffn, dg_v[...])) * dot_nt(ffn, du_v[...])).astype(BF16)
    logit = jnp.sum(hidden.astype(F32) * gate_vector[...], axis=-1, keepdims=True)
    l_send[...] = jnp.broadcast_to(logit, l_send.shape)
    @pl.loop(0, n_outer - 1)
    def _(k):
        s = 2 * near_first(k) + inner
        ag_arrival(s).wait_recv()
        pair_copy(s).start()
        fw_copy(s).start()

    for j in range(n_tp):
        dense_out_copies[j].wait()
        d_send[j] = dot(hidden, dd_v[j]).astype(BF16)

    def ds_copies(d):
        peer = lax.rem(mt + d, n_tp)
        return (
            pltpu.make_async_remote_copy(
                d_send.at[peer], d_recv.at[mt], ds_ss.at[peer], ds_rs.at[mt],
                device_id={"tp": peer}, device_id_type=MESH,
            ),
            pltpu.make_async_remote_copy(
                l_send, l_recv.at[mt], lg_ss.at[peer], lg_rs.at[mt], device_id={"tp": peer}, device_id_type=MESH
            ),
        )

    def ds_arrivals(d):
        peer = lax.rem(mt + d, n_tp)
        return (
            pltpu.make_async_remote_copy(
                d_send.at[peer], d_recv.at[peer], ds_ss.at[peer], ds_rs.at[peer],
                device_id={"tp": peer}, device_id_type=MESH,
            ),
            pltpu.make_async_remote_copy(
                l_send, l_recv.at[peer], lg_ss.at[peer], lg_rs.at[peer], device_id={"tp": peer}, device_id_type=MESH
            ),
        )

    for d in range(1, n_tp):
        for copy in ds_copies(d):
            copy.start()

    @pl.loop(0, n_outer)
    def _(k):
        o = jnp.where(k == 0, outer, near_first(jnp.maximum(k - 1, 0)))
        s = 2 * o + 1 - inner
        ag_arrival(s).wait_recv()
        fw_copy(s).start()

    for copy in expert_in:
        copy.wait()
    for copy in expert_out:
        copy.wait()

    @pl.loop(1, n_ep)
    def _(d):
        fw_arrival(lax.rem(me + n_ep - d, n_ep)).wait_recv()

    span = min(n_ep, 8)
    rows = span * n_seq

    @pl.loop(0, n_ep // span)
    def _(i):
        groups = pl.ds(i * span, span)
        low = gathered[0, groups].reshape(rows, half)
        high = gathered[1, groups].reshape(rows, half)
        pre = dot(low, wg_v[:half, :]) + dot(high, wg_v[half:, :])
        upper = dot(low, wu_v[:half, :]) + dot(high, wu_v[half:, :])
        act = (silu(pre) * upper).astype(BF16)
        for j in range(n_tp):
            p_send[j % 2, j // 2, groups] = dot(act, wd_v[j]).astype(BF16).reshape(span, n_seq, cols)

    def near_copy(x, g):
        return pltpu.make_async_remote_copy(
            p_send.at[1 - side, x, g], n_recv.at[x, g], p_ss.at[x, g], p_rs.at[x, g],
            device_id={"tp": partner}, device_id_type=MESH,
        )

    def far_copy(d, g):
        x = lax.rem(far + d, n_far)
        return pltpu.make_async_remote_copy(
            x_send.at[x, g], x_recv.at[far, g], x_ss.at[x, g], x_rs.at[far, g],
            device_id={"tp": 2 * x + side}, device_id_type=MESH,
        )

    def far_arrival(d, g):
        x = lax.rem(far + d, n_far)
        return pltpu.make_async_remote_copy(
            x_send.at[x, g], x_recv.at[x, g], x_ss.at[x, g], x_rs.at[x, g],
            device_id={"tp": 2 * x + side}, device_id_type=MESH,
        )

    def e_copy(g):
        return pltpu.make_async_remote_copy(
            e_send.at[g], e_recv.at[me], e_ss.at[g], e_rs.at[me], device_id={"ep": g}, device_id_type=MESH
        )

    def e_arrival(g):
        return pltpu.make_async_remote_copy(
            e_send.at[g], e_recv.at[g], e_ss.at[g], e_rs.at[g], device_id={"ep": g}, device_id_type=MESH
        )

    @pl.loop(0, n_ep)
    def _(k):
        g = group_at(k)
        for d in range(1, n_far + 1):
            near_copy(lax.rem(far + d, n_far), g).start()

    def pair_sum(x, g):
        near_copy(x, g).wait_recv()
        return p_send[side, x, g].astype(F32) + n_recv[x, g].astype(F32)

    @pl.loop(0, n_ep)
    def _(k):
        g = group_at(k)
        for d in range(1, n_far):
            x = lax.rem(far + d, n_far)
            x_send[x, g] = pair_sum(x, g).astype(BF16)
            far_copy(d, g).start()

    def summed(g):
        total = pair_sum(far, g)
        for d in range(1, n_far):
            far_arrival(d, g).wait_recv()
            total = total + x_recv[lax.rem(far + d, n_far), g].astype(F32)
        return total.astype(BF16)

    @pl.loop(0, n_ep - 1)
    def _(k):
        g = group_at(k)
        e_send[g] = summed(g)
        e_copy(g).start()

    e_recv[me] = summed(me)

    dense_sum = d_send[mt].astype(F32)
    logit_sum = l_send[...]
    for d in range(1, n_tp):
        for copy in ds_arrivals(d):
            copy.wait_recv()
        peer = lax.rem(mt + d, n_tp)
        dense_sum = dense_sum + d_recv[peer].astype(F32)
        logit_sum = logit_sum + l_recv[peer]
    gate = 1.0 / (1.0 + jnp.exp(-logit_sum[:, 0:1]))
    total = residual[mt] + gate * dense_sum

    eye = lax.broadcasted_iota(jnp.int32, (n_seq, n_seq), 0) == lax.broadcasted_iota(jnp.int32, (n_seq, n_seq), 1)

    def column(row):
        return jnp.sum(jnp.where(eye, row, 0.0), axis=1, keepdims=True)

    route_columns = [column(routes_t[k:k + 1, :].astype(F32)) for k in range(TOPK)]
    weight_columns = [column(weight_t[k:k + 1, :]) for k in range(TOPK)]

    def add_expert(e, acc):
        coef = jnp.zeros((n_seq, 1), F32)
        number = jnp.full((n_seq, 1), e, jnp.int32).astype(F32)
        for k in range(TOPK):
            coef = coef + jnp.where(route_columns[k] == number, weight_columns[k], 0.0)
        return acc + coef * e_recv[e].astype(F32)

    total = add_expert(me, total)

    def receive(d, acc):
        e = lax.rem(me + n_ep - d, n_ep)
        e_arrival(e).wait_recv()
        return add_expert(e, acc)

    total = lax.fori_loop(1, n_ep, receive, total)
    out[...] = total.astype(BF16)

    for d in range(1, n_tp):
        ar_copy(d).wait_send()
        for copy in ds_copies(d):
            copy.wait_send()

    @pl.loop(1, n_ep)
    def _(d):
        g = lax.rem(me + d, n_ep)
        fw_copy(g).wait_send()
        e_copy(g).wait_send()

    pair_copy(me).wait_send()

    @pl.loop(1, n_outer)
    def _(d):
        ag_copy(d - 1).wait_send()
        pair_copy(lax.rem(me + 2 * d, n_ep)).wait_send()

    @pl.loop(0, n_ep)
    def _(g):
        for x in range(n_far):
            near_copy(x, g).wait_send()
        for d in range(1, n_far):
            far_copy(d, g).wait_send()


def shards(
    tokens, norm_gain, query_weight, key_weight, value_weight, output_weight, head_gain, lambdas,
    key_cache, value_cache, lengths, ffn_gain, routes, route_weight, expert_gate, expert_up,
    expert_down, dense_gate, dense_up, dense_down, gate_vector,
):
    n_ep, n_tp = lax.axis_size("ep"), lax.axis_size("tp")
    n_seq, width = tokens.shape
    cols = width // n_tp
    half = width // 2
    cache_len = key_cache.shape[1]
    keys = key_cache.reshape(n_seq, cache_len, 2 * DQK)
    values = value_cache.reshape(n_seq, cache_len, DV)
    hid = expert_gate.shape[2]
    dense = dense_gate.shape[0]
    vmem = pl.BlockSpec(memory_space=pltpu.VMEM)
    smem = pl.BlockSpec(memory_space=pltpu.SMEM)
    hbm = pl.BlockSpec(memory_space=pl.ANY)

    def held(*shape, dtype=BF16):
        return pltpu.VMEM(shape, dtype)

    def sems(*shape):
        return pltpu.SemaphoreType.DMA(shape)

    return pl.pallas_call(
        functools.partial(layer_kernel, n_ep, n_tp),
        out_shape=jax.ShapeDtypeStruct((n_seq, cols), BF16),
        in_specs=[smem] * 2 + [vmem] * 7 + [hbm] * 12,
        out_specs=vmem,
        scratch_shapes=[
            held(*query_weight.shape), held(*key_weight.shape), held(*value_weight.shape), held(*output_weight.shape),
            held(*keys.shape), held(*values.shape),
            held(width, hid), held(width, hid), held(n_tp, hid, cols),
            held(dense, width), held(dense, width), held(n_tp, dense, cols),
            held(n_seq, 8, 2 * DQK, dtype=F32), held(n_seq, 1, 2 * DQK, dtype=F32),
            held(n_seq, 1, DV, dtype=F32), held(n_seq, 8, DV, dtype=F32),
            held(n_seq, width), held(n_tp, n_seq, width), held(n_tp, n_seq, cols, dtype=F32),
            held(2, n_ep, n_seq, half),
            held(n_tp, n_seq, cols), held(n_tp, n_seq, cols),
            held(n_seq, 128, dtype=F32), held(n_tp, n_seq, 128, dtype=F32),
            held(2, n_tp // 2, n_ep, n_seq, cols), held(n_tp // 2, n_ep, n_seq, cols),
            held(n_tp // 2, n_ep, n_seq, cols), held(n_tp // 2, n_ep, n_seq, cols),
            held(n_ep, n_seq, cols), held(n_ep, n_seq, cols),
            sems(8), sems(n_seq // SEQ_CHUNK), sems(n_seq // SEQ_CHUNK), sems(n_tp), sems(n_tp),
            sems(n_tp), sems(n_tp), sems(n_ep), sems(n_ep), sems(n_ep), sems(n_ep),
            sems(n_tp), sems(n_tp), sems(n_tp), sems(n_tp),
            sems(n_tp // 2, n_ep), sems(n_tp // 2, n_ep), sems(n_tp // 2, n_ep), sems(n_tp // 2, n_ep), sems(n_ep), sems(n_ep),
            sems(n_ep),
        ],
        compiler_params=pltpu.CompilerParams(
            collective_id=0, has_side_effects=True, vmem_limit_bytes=58 * 1024 * 1024
        ),
    )(
        lengths, lambdas,
        tokens, norm_gain[None, :], head_gain[None, :], ffn_gain[None, :], gate_vector[None, :],
        routes.T, route_weight.T,
        query_weight, key_weight, value_weight, output_weight, keys, values,
        expert_gate[0], expert_up[0], expert_down[0], dense_gate, dense_up, dense_down,
    )


def solution(mesh):
    placed = (
        P("ep", None),
        P(),
        P(None, "tp"),
        P(None, "tp"),
        P(None, "tp"),
        P("tp", None),
        P(),
        P("tp"),
        P("ep", None, "tp", None),
        P("ep", None, "tp", None),
        P("ep"),
        P(),
        P("ep", None),
        P("ep", None),
        P("ep", None, "tp"),
        P("ep", None, "tp"),
        P("ep", "tp", None),
        P("tp", None),
        P("tp", None),
        P("tp", None),
        P("tp"),
    )
    return jax.shard_map(
        shards, mesh=mesh, in_specs=placed, out_specs=P("ep", "tp"), check_vma=False
    )
```

profile of v0, /device:TPU:0, one launch (start us, length us, event | category | flops | bytes accessed | tf_op | source)
XLA Modules:
  0.0 36.3 jit_solution(13445558577128884994)
XLA Ops:
  0.0 35.0 %shard_map.199 = bf16[16,512]{1,0:T(8,128)(2,1)} custom-call(s32[16]{0:T(128)} %lengths.1, f32[2]{0:T(128)} %lambdas.1, bf16[16,2048]{1,0:T(8,128)(2,1)} %tokens.1, f32[1,2048]{1,0:T(1,128)} %bitcast.16, f32[1,128]{1,0:T(1,128)} %bitcast.21, f32[1,2048]{1,0:T(1,128)} %bitcast.17, f32[1,512]{1,0:T(1,128)} %bitcast.18, s32[4,16]{1,0:T(4,128)} %bitcast.19, ...), custom_call_target="tpu_custom_call" | custom-call | tf_op jit(solution)/shard_map/pallas_call | solution.py:452
  35.0 1.3 %copy.23 = bf16[16,512]{1,0:T(8,128)(2,1)} copy(bf16[16,512]{1,0:T(8,128)(2,1)} %shard_map.199) | data formatting | bytes 32768
where the time goes:
time: 36.6 us; the launch traced here: 36.3 us
  Pallas kernels  35 us (96%)
  local copies, waits for them, and re-layouts  1.32 us (4%)
    pallas_call x1, Pallas kernels, shards(): pl.pallas_call(functools.partial(layer_kernel, n_ep, n_tp), out_shape=jax...  35 us
    unnamed x1, local copies, waits for them, and re-layouts  1.32 us

commit v1 on v0

--- a/solution.py
+++ b/solution.py
@@ -38,18 +38,18 @@
 
 def layer_kernel(
     n_ep, n_tp,
-    lengths, lambdas,
-    tokens, norm_gain, head_gain, ffn_gain, gate_vector, routes_t, weight_t,
+    lengths_h, lambdas_h,
+    tokens_h, norm_gain_h, head_gain_h, ffn_gain_h, gate_vector_h, routes_h, weight_h,
     wq, wk, wv, wo, key_cache, value_cache, wg, wu, wd, dg, du, dd,
     out,
+    lengths, lambdas, tokens, norm_gain, head_gain, ffn_gain, gate_vector, routes_t, weight_t,
     wq_v, wk_v, wv_v, wo_v, key_v, value_v, wg_v, wu_v, wd_v, dg_v, du_v, dd_v,
     q_rows, k_rows, v_rows, mix,
     ar_send, ar_recv, residual, gathered,
     d_send, d_recv, l_send, l_recv,
     p_send, n_recv, x_send, x_recv, e_send, e_recv,
-    load_sem, key_sem, value_sem, wd_sem, dd_sem,
+    small_sem, load_sem, cache_sem,
     ar_ss, ar_rs, ag_ss, ag_rs, fw_ss, fw_rs, ds_ss, ds_rs, lg_ss, lg_rs, p_ss, p_rs, x_ss, x_rs, e_ss, e_rs,
-    pair_ss,
 ):
     me = lax.axis_index("ep")
     mt = lax.axis_index("tp")
@@ -89,20 +89,28 @@
         copy.start()
         return copy
 
+    small = [
+        load(src, dst, small_sem.at[i]) for i, (src, dst) in enumerate((
+            (tokens_h, tokens), (norm_gain_h, norm_gain), (lambdas_h, lambdas), (lengths_h, lengths),
+            (head_gain_h, head_gain), (ffn_gain_h, ffn_gain), (gate_vector_h, gate_vector),
+            (routes_h, routes_t), (weight_h, weight_t),
+        ))
+    ]
     first = [load(wq, wq_v, load_sem.at[0]), load(wk, wk_v, load_sem.at[1]), load(wv, wv_v, load_sem.at[2])]
     n_chunk = n_seq // SEQ_CHUNK
 
     def cache_copies(i):
         rows = pl.ds(i * SEQ_CHUNK, SEQ_CHUNK)
         return (
-            pltpu.make_async_copy(key_cache.at[rows], key_v.at[rows], key_sem.at[i]),
-            pltpu.make_async_copy(value_cache.at[rows], value_v.at[rows], value_sem.at[i]),
-        )
-
-    for i in range(n_chunk):
+            pltpu.make_async_copy(key_cache.at[rows], key_v.at[rows], cache_sem.at[2 * i]),
+            pltpu.make_async_copy(value_cache.at[rows], value_v.at[rows], cache_sem.at[2 * i + 1]),
+        )
+
+    def start_cache(i):
         for copy in cache_copies(i):
             copy.start()
-    wo_copy = load(wo, wo_v, load_sem.at[3])
+
+    start_cache(0)
     barrier = pltpu.get_barrier_semaphore()
     for d in range(1, n_tp):
         pl.semaphore_signal(barrier, inc=1, device_id={"tp": lax.rem(mt + d, n_tp)}, device_id_type=MESH)
@@ -111,9 +119,17 @@
     def _(d):
         pl.semaphore_signal(barrier, inc=1, device_id={"ep": lax.rem(me + d, n_ep)}, device_id_type=MESH)
 
+    for copy in small[:2]:
+        copy.wait()
     wide = tokens[...].astype(F32)
     normed = rms_scale(wide, norm_gain[...]).astype(BF16)
-    for copy in first:
+    first[0].wait()
+    for i in range(1, n_chunk):
+        start_cache(i)
+    wo_copy = load(wo, wo_v, load_sem.at[3])
+    for copy in first[1:]:
+        copy.wait()
+    for copy in small[2:4]:
         copy.wait()
     q = dot(normed, wq_v[...]).astype(BF16).astype(F32)
     k_rows[:, 0, :] = dot(normed, wk_v[...]).astype(BF16).astype(F32)
@@ -154,10 +170,12 @@
             mix[n] = m
 
     dense_in = [load(dg, dg_v, load_sem.at[4]), load(du, du_v, load_sem.at[5])]
-    dense_out_copies = [load(dd.at[:, pl.ds(j * cols, cols)], dd_v.at[j], dd_sem.at[j]) for j in range(n_tp)]
+    dense_out_copies = [load(dd.at[:, pl.ds(j * cols, cols)], dd_v.at[j], load_sem.at[8 + j]) for j in range(n_tp)]
     expert_in = [load(wg, wg_v, load_sem.at[6]), load(wu, wu_v, load_sem.at[7])]
-    expert_out = [load(wd.at[:, pl.ds(j * cols, cols)], wd_v.at[j], wd_sem.at[j]) for j in range(n_tp)]
-
+    expert_out = [load(wd.at[:, pl.ds(j * cols, cols)], wd_v.at[j], load_sem.at[8 + n_tp + j]) for j in range(n_tp)]
+
+    for copy in small[4:]:
+        copy.wait()
     heads = [rms_scale(mix[:, h, :], head_gain[...]).astype(BF16) for h in range(group)]
     wo_copy.wait()
     partial = dot(heads[0], wo_v[0:DV, :])
@@ -170,13 +188,13 @@
     def ar_copy(d):
         peer = lax.rem(mt + d, n_tp)
         return pltpu.make_async_remote_copy(
-            ar_send, ar_recv.at[mt], ar_ss.at[peer], ar_rs.at[mt], device_id={"tp": peer}, device_id_type=MESH
+            ar_send, ar_recv.at[mt], ar_ss.at[0], ar_rs.at[mt], device_id={"tp": peer}, device_id_type=MESH
         )
 
     def ar_arrival(d):
         peer = lax.rem(mt + d, n_tp)
         return pltpu.make_async_remote_copy(
-            ar_send, ar_recv.at[peer], ar_ss.at[peer], ar_rs.at[peer], device_id={"tp": peer}, device_id_type=MESH
+            ar_send, ar_recv.at[peer], ar_ss.at[0], ar_rs.at[peer], device_id={"tp": peer}, device_id_type=MESH
         )
 
     for d in range(1, n_tp):
@@ -200,23 +218,23 @@
 
     def ag_copy(k):
         peer = 2 * far_first(k) + inner
-        return ag_piece(peer, me, ag_ss.at[peer])
+        return ag_piece(peer, me, ag_ss.at[0])
 
     def pair_copy(s):
-        return ag_piece(across, s, pair_ss.at[s])
+        return ag_piece(across, s, ag_ss.at[0])
 
     def ag_arrival(s):
-        return ag_piece(across, s, ag_ss.at[s])
+        return ag_piece(across, s, ag_ss.at[0])
 
     def fw_copy(s):
         return pltpu.make_async_remote_copy(
-            gathered.at[side, s], gathered.at[side, s], fw_ss.at[s], fw_rs.at[s],
+            gathered.at[side, s], gathered.at[side, s], fw_ss.at[0], fw_rs.at[s],
             device_id={"tp": partner}, device_id_type=MESH,
         )
 
     def fw_arrival(s):
         return pltpu.make_async_remote_copy(
-            gathered.at[1 - side, s], gathered.at[1 - side, s], fw_ss.at[s], fw_rs.at[s],
+            gathered.at[1 - side, s], gathered.at[1 - side, s], fw_ss.at[0], fw_rs.at[s],
             device_id={"tp": partner}, device_id_type=MESH,
         )
 
@@ -246,11 +264,11 @@
         peer = lax.rem(mt + d, n_tp)
         return (
             pltpu.make_async_remote_copy(
-                d_send.at[peer], d_recv.at[mt], ds_ss.at[peer], ds_rs.at[mt],
+                d_send.at[peer], d_recv.at[mt], ds_ss.at[0], ds_rs.at[mt],
                 device_id={"tp": peer}, device_id_type=MESH,
             ),
             pltpu.make_async_remote_copy(
-                l_send, l_recv.at[mt], lg_ss.at[peer], lg_rs.at[mt], device_id={"tp": peer}, device_id_type=MESH
+                l_send, l_recv.at[mt], lg_ss.at[0], lg_rs.at[mt], device_id={"tp": peer}, device_id_type=MESH
             ),
         )
 
@@ -258,11 +276,11 @@
         peer = lax.rem(mt + d, n_tp)
         return (
             pltpu.make_async_remote_copy(
-                d_send.at[peer], d_recv.at[peer], ds_ss.at[peer], ds_rs.at[peer],
+                d_send.at[peer], d_recv.at[peer], ds_ss.at[0], ds_rs.at[peer],
                 device_id={"tp": peer}, device_id_type=MESH,
             ),
             pltpu.make_async_remote_copy(
-                l_send, l_recv.at[peer], lg_ss.at[peer], lg_rs.at[peer], device_id={"tp": peer}, device_id_type=MESH
+                l_send, l_recv.at[peer], lg_ss.at[0], lg_rs.at[peer], device_id={"tp": peer}, device_id_type=MESH
             ),
         )
 
@@ -302,32 +320,32 @@
 
     def near_copy(x, g):
         return pltpu.make_async_remote_copy(
-            p_send.at[1 - side, x, g], n_recv.at[x, g], p_ss.at[x, g], p_rs.at[x, g],
+            p_send.at[1 - side, x, g], n_recv.at[x, g], p_ss.at[0], p_rs.at[x, g],
             device_id={"tp": partner}, device_id_type=MESH,
         )
 
     def far_copy(d, g):
         x = lax.rem(far + d, n_far)
         return pltpu.make_async_remote_copy(
-            x_send.at[x, g], x_recv.at[far, g], x_ss.at[x, g], x_rs.at[far, g],
+            x_send.at[x, g], x_recv.at[far, g], x_ss.at[0], x_rs.at[far, g],
             device_id={"tp": 2 * x + side}, device_id_type=MESH,
         )
 
     def far_arrival(d, g):
         x = lax.rem(far + d, n_far)
         return pltpu.make_async_remote_copy(
-            x_send.at[x, g], x_recv.at[x, g], x_ss.at[x, g], x_rs.at[x, g],
+            x_send.at[x, g], x_recv.at[x, g], x_ss.at[0], x_rs.at[x, g],
             device_id={"tp": 2 * x + side}, device_id_type=MESH,
         )
 
     def e_copy(g):
         return pltpu.make_async_remote_copy(
-            e_send.at[g], e_recv.at[me], e_ss.at[g], e_rs.at[me], device_id={"ep": g}, device_id_type=MESH
+            e_send.at[g], e_recv.at[me], e_ss.at[0], e_rs.at[me], device_id={"ep": g}, device_id_type=MESH
         )
 
     def e_arrival(g):
         return pltpu.make_async_remote_copy(
-            e_send.at[g], e_recv.at[g], e_ss.at[g], e_rs.at[g], device_id={"ep": g}, device_id_type=MESH
+            e_send.at[g], e_recv.at[g], e_ss.at[0], e_rs.at[g], device_id={"ep": g}, device_id_type=MESH
         )
 
     @pl.loop(0, n_ep)
@@ -399,30 +417,17 @@
     total = lax.fori_loop(1, n_ep, receive, total)
     out[...] = total.astype(BF16)
 
-    for d in range(1, n_tp):
-        ar_copy(d).wait_send()
-        for copy in ds_copies(d):
-            copy.wait_send()
-
-    @pl.loop(1, n_ep)
-    def _(d):
-        g = lax.rem(me + d, n_ep)
-        fw_copy(g).wait_send()
-        e_copy(g).wait_send()
-
-    pair_copy(me).wait_send()
-
-    @pl.loop(1, n_outer)
-    def _(d):
-        ag_copy(d - 1).wait_send()
-        pair_copy(lax.rem(me + 2 * d, n_ep)).wait_send()
-
-    @pl.loop(0, n_ep)
-    def _(g):
-        for x in range(n_far):
-            near_copy(x, g).wait_send()
-        for d in range(1, n_far):
-            far_copy(d, g).wait_send()
+    def drain(ref, sem):
+        pltpu.make_async_copy(ref, ref, sem.at[0]).wait()
+
+    drain(ar_recv.at[pl.ds(0, n_tp - 1)], ar_ss)
+    drain(d_recv.at[pl.ds(0, n_tp - 1)], ds_ss)
+    drain(l_recv.at[pl.ds(0, n_tp - 1)], lg_ss)
+    drain(gathered.at[0, pl.ds(0, n_ep - 1)], ag_ss)
+    drain(gathered.at[1, pl.ds(0, n_ep - 1)], fw_ss)
+    drain(n_recv, p_ss)
+    drain(x_send.at[pl.ds(0, n_far - 1)], x_ss)
+    drain(e_send.at[pl.ds(0, n_ep - 1)], e_ss)
 
 
 def shards(
@@ -440,7 +445,6 @@
     hid = expert_gate.shape[2]
     dense = dense_gate.shape[0]
     vmem = pl.BlockSpec(memory_space=pltpu.VMEM)
-    smem = pl.BlockSpec(memory_space=pltpu.SMEM)
     hbm = pl.BlockSpec(memory_space=pl.ANY)
 
     def held(*shape, dtype=BF16):
@@ -451,10 +455,14 @@
 
     return pl.pallas_call(
         functools.partial(layer_kernel, n_ep, n_tp),
-        out_shape=jax.ShapeDtypeStruct((n_seq, cols), BF16),
-        in_specs=[smem] * 2 + [vmem] * 7 + [hbm] * 12,
+        out_shape=pltpu.VMEM((n_seq, cols), BF16),
+        in_specs=[hbm] * 21,
         out_specs=vmem,
         scratch_shapes=[
+            pltpu.SMEM(lengths.shape, jnp.int32), pltpu.SMEM(lambdas.shape, F32),
+            held(n_seq, width), held(1, width, dtype=F32), held(1, head_gain.shape[0], dtype=F32),
+            held(1, width, dtype=F32), held(1, dense, dtype=F32), held(TOPK, n_seq, dtype=jnp.int32),
+            held(TOPK, n_seq, dtype=F32),
             held(*query_weight.shape), held(*key_weight.shape), held(*value_weight.shape), held(*output_weight.shape),
             held(*keys.shape), held(*values.shape),
             held(width, hid), held(width, hid), held(n_tp, hid, cols),
@@ -468,11 +476,10 @@
             held(2, n_tp // 2, n_ep, n_seq, cols), held(n_tp // 2, n_ep, n_seq, cols),
             held(n_tp // 2, n_ep, n_seq, cols), held(n_tp // 2, n_ep, n_seq, cols),
             held(n_ep, n_seq, cols), held(n_ep, n_seq, cols),
-            sems(8), sems(n_seq // SEQ_CHUNK), sems(n_seq // SEQ_CHUNK), sems(n_tp), sems(n_tp),
-            sems(n_tp), sems(n_tp), sems(n_ep), sems(n_ep), sems(n_ep), sems(n_ep),
-            sems(n_tp), sems(n_tp), sems(n_tp), sems(n_tp),
-            sems(n_tp // 2, n_ep), sems(n_tp // 2, n_ep), sems(n_tp // 2, n_ep), sems(n_tp // 2, n_ep), sems(n_ep), sems(n_ep),
-            sems(n_ep),
+            sems(9), sems(8 + 2 * n_tp), sems(2 * (n_seq // SEQ_CHUNK)),
+            sems(1), sems(n_tp), sems(1), sems(n_ep), sems(1), sems(n_ep),
+            sems(1), sems(n_tp), sems(1), sems(n_tp),
+            sems(1), sems(n_tp // 2, n_ep), sems(1), sems(n_tp // 2, n_ep), sems(1), sems(n_ep),
         ],
         compiler_params=pltpu.CompilerParams(
             collective_id=0, has_side_effects=True, vmem_limit_bytes=58 * 1024 * 1024

time: 36.6 us -> 32.7 us (0.89)
  Pallas kernels: 35 us -> 32 us
  local copies, waits for them, and re-layouts: 1.32 us -> 0.61 us
    pallas_call x1, Pallas kernels: 35 us -> 32 us  [shards(): pl.pallas_call(functools.partial(layer_kernel, n_ep, n_tp), out_shape=plt...]
    unnamed x1, local copies, waits for them, and re-layouts: 1.32 us -> 0.61 us
where the time goes in v1:
time: 32.7 us; the launch traced here: 32.6 us
  Pallas kernels  32 us (98%)
  local copies, waits for them, and re-layouts  0.61 us (2%)
    pallas_call x1, Pallas kernels, shards(): pl.pallas_call(functools.partial(layer_kernel, n_ep, n_tp), out_shape=plt...  32 us

profile of v1, /device:TPU:0, one launch (start us, length us, event | category | flops | bytes accessed | tf_op | source)
XLA Modules:
  0.0 32.6 jit_solution(6369837154544754039)
XLA Ops:
  0.0 32.0 %shard_map.199 = bf16[16,512]{1,0:T(8,128)(2,1)S(1)} custom-call(s32[16]{0:T(128)} %lengths_h.1, f32[2]{0:T(128)} %lambdas_h.1, bf16[16,2048]{1,0:T(8,128)(2,1)} %tokens_h.1, f32[1,2048]{1,0:T(1,128)} %bitcast.16, f32[1,128]{1,0:T(1,128)} %bitcast.21, f32[1,2048]{1,0:T(1,128)} %bitcast.17, f32[1,512]{1,0:T(1,128)} %bitcast.18, s32[4,16]{1,0:T(4,128)} %bitcast.19, ...), custom_call_target="tpu_custom_call" | custom-call | tf_op jit(solution)/shard_map/pallas_call | solution.py:456
  32.0 0.6 %copy.23 = bf16[16,512]{1,0:T(8,128)(2,1)} copy(bf16[16,512]{1,0:T(8,128)(2,1)S(1)} %shard_map.199) | data formatting | bytes 32768
